TPU v7x, 256 devices: a whole 4x4x8 slice. The times are simulated.
256 devices in a mesh: kv: 16 (over y, x), tp: 16 (over z, core).
Axes of the slice: x: 4, y: 4, z: 8, core: 2. Of those that a mesh axis runs over, the one named last changes fastest.
Arguments:
- tokens: bfloat16 [1024, 4096], P('tp', 'kv'), may hold values from -19 to 19, as said below
- lengths: int32 [1024], P('kv'), may hold values from 1 to 16384, 4194304 in all
- state_block: float32 [1024, 64, 2048], P('kv', None, 'tp'), may hold values from -6 to 6
- cached_keys: bfloat16 [1024, 128, 2048], P('kv', None, 'tp'), may hold values from -0.75 to 0.75
- cached_values: bfloat16 [1024, 128, 2048], P('kv', None, 'tp'), may hold values from -6 to 6
- query_weight: bfloat16 [4096, 2048], P('kv', 'tp'), may hold values from -0.09375 to 0.09375
- key_weight: bfloat16 [4096, 2048], P('kv', 'tp'), may hold values from -0.09375 to 0.09375
- value_weight: bfloat16 [4096, 2048], P('kv', 'tp'), may hold values from -0.09375 to 0.09375
- gate_weight: bfloat16 [4096, 2048], P('kv', 'tp'), may hold values from -0.09375 to 0.09375
- decay_rate: float32 [32], P('tp'), may hold values from 0.0005 to 0.05
- head_gain: float32 [2048], P('tp'), may hold values from 0.1 to 1.9
- out_weight: bfloat16 [2048, 4096], P('tp', 'kv'), may hold values from -0.125 to 0.125
- mixer_gain: float32 [4096], P('kv'), may hold values from 0.1 to 1.9
- up_weight: bfloat16 [4096, 16384], P('kv', 'tp'), may hold values from -0.09375 to 0.09375
- down_weight: bfloat16 [16384, 4096], P('tp', 'kv'), may hold values from -0.046875 to 0.046875
- final_gain: float32 [4096], P('kv'), may hold values from 0.1 to 1.9
Outputs:
- next_rows: bfloat16 [1024, 4096], P('tp', 'kv')
Inputs may be any that keep to these rules, and one draw needn't show every extreme that they name: `tokens`: the rows' column groups have scales that differ between groups.
All inputs are finite; a program needn't handle non-finite values. No bound on the sum of `lengths` on one device may be relied on, other than what follows from the above.
Results may differ from a plain program's by a relative error of at most 0.0095.
Values may be sent and summed in bfloat16 or wider, within the bound.
No kernel may reach another device: no remote copies, remote signals or barrier semaphores. Data moves between devices by JAX's collectives and lax.ppermute only.
A program may use at most 64 MiB of HBM per device.

v0:
```python
import functools

import jax
import jax.numpy as jnp
from jax import lax
from jax.sharding import Mesh
from jax.sharding import PartitionSpec as P

HDIM = 64
BLK = 128
KV = ("kv_0", "kv_1")


ALPHA = 2.0**0.5
EPS = 1e-05


def by_axis(x, axes):
    return functools.reduce(lax.psum, axes, x)


def copy_for_each(x, axis):
    peers = lax.axis_size(axis)
    return lax.all_to_all(jnp.broadcast_to(x[None], (peers, *x.shape)), axis, 0, 0, tiled=True)


def joined_along(parts, dim):
    parts = jnp.moveaxis(parts, 0, dim)
    dims = parts.shape
    return parts.reshape(*dims[:dim], dims[dim] * dims[dim + 1], *dims[dim + 2 :])


def gather_directly(x, axis, dim):
    parts = copy_for_each(x, axis)
    return joined_along(parts, dim)


def split_up(x, dim, peers):
    dims = x.shape
    parts = x.reshape(*dims[:dim], peers, dims[dim] // peers, *dims[dim + 1 :])
    return jnp.moveaxis(parts, dim, 0)


def sent_and_summed(x, axis, dim):
    parts = split_up(x, dim, lax.axis_size(axis))
    arrived = lax.all_to_all(parts, axis, split_axis=0, concat_axis=0, tiled=True)
    return arrived.sum(axis=0)


def rotate(vectors, positions):
    half = vectors.shape[-1] // 2
    inverse = 10000.0 ** (-jnp.arange(half, dtype=jnp.float32) / half)
    angle = positions.astype(jnp.float32)[:, None] * inverse[None, :]
    cosine = jnp.cos(angle)[:, None, :]
    sine = jnp.sin(angle)[:, None, :]
    former, latter = (vectors[..., :half], vectors[..., half:])
    return jnp.concatenate([former * cosine - latter * sine, latter * cosine + former * sine], -1)


def normalize(values, gain):
    width = values.shape[1] * lax.axis_size(KV)
    total, square = (by_axis(jnp.sum(values, 1), KV), by_axis(jnp.sum(values * values, 1), KV))
    mean = total / width
    centred = values - mean[:, None]
    spread = square / width - mean * mean
    return centred * lax.rsqrt(spread[:, None] + EPS) * gain[None, :]


def retain(query, keyed, valued, gated, lengths, state, keys, values, rate, gain):
    count = query.shape[0]
    heads = rate.shape[0]
    q_rot = rotate(query.astype(jnp.float32).reshape(count, heads, HDIM), lengths).astype(
        jnp.bfloat16
    )
    k_rot = (rotate(keyed.astype(jnp.float32).reshape(count, heads, HDIM), lengths) * 0.125).astype(
        jnp.bfloat16
    )
    v_new = valued.astype(jnp.float32).reshape(count, heads, HDIM)
    cached_k = keys.reshape(count, BLK, heads, HDIM)
    cached_v = values.reshape(count, BLK, heads, HDIM)
    scores = jnp.einsum("shn,sihn->shi", q_rot, cached_k, preferred_element_type=jnp.float32)
    offset = lengths % BLK
    slots = jnp.arange(BLK, dtype=jnp.int32)
    lag = jnp.maximum(offset[:, None] - slots[None, :], 0).astype(jnp.float32)
    live = (slots[None, :] < offset[:, None])[:, None, :]
    factor = jnp.where(live, jnp.exp(-rate[None, :, None] * lag[:, None, :]), 0.0)
    weights = (scores * factor).astype(jnp.bfloat16)
    own = jnp.einsum("shn,shn->sh", q_rot, k_rot, preferred_element_type=jnp.float32).astype(
        jnp.bfloat16
    )
    inner = jnp.einsum("shi,sihn->shn", weights, cached_v, preferred_element_type=jnp.float32)
    inner = inner + own.astype(jnp.float32)[..., None] * v_new
    carried = jnp.exp(-rate[None, :] * (offset[:, None] + 1).astype(jnp.float32))
    cross = (
        jnp.einsum(
            "shk,skhv->shv", q_rot.astype(jnp.float32), state.reshape(count, HDIM, heads, HDIM)
        )
        * carried[..., None]
    )
    retained = inner + cross
    mean = jnp.mean(retained, -1, keepdims=True)
    centred = retained - mean
    spread = jnp.mean(centred * centred, -1, keepdims=True)
    normed = centred * lax.rsqrt(spread + EPS) * gain.reshape(heads, HDIM)[None]
    gate_f = jax.nn.silu(gated.astype(jnp.float32).reshape(count, heads, HDIM))
    return (gate_f * normed).reshape(count, heads * HDIM).astype(jnp.bfloat16)


def per_device(
    tokens,
    lengths,
    state_block,
    cached_keys,
    cached_values,
    query_weight,
    key_weight,
    value_weight,
    gate_weight,
    decay_rate,
    head_gain,
    out_weight,
    mixer_gain,
    up_weight,
    down_weight,
    final_gain,
):
    all_rows = gather_directly(tokens, "tp", 0)
    width = query_weight.shape[1]
    piece = all_rows
    summed = sent_and_summed(
        jnp.concatenate(
            [
                jnp.dot(piece, weight, preferred_element_type=jnp.float32)
                for weight in (query_weight, key_weight, value_weight, gate_weight)
            ],
            1,
        ),
        KV,
        0,
    ).astype(jnp.bfloat16)
    query, keyed, valued, gated = [
        summed[:, index * width : (index + 1) * width] for index in range(4)
    ]
    mixed = retain(
        query,
        keyed,
        valued,
        gated,
        lengths,
        state_block,
        cached_keys,
        cached_values,
        decay_rate,
        head_gain,
    )
    mixed_all = gather_directly(mixed, KV, 0)
    piece = mixed_all
    branch = sent_and_summed(
        jnp.dot(piece, out_weight, preferred_element_type=jnp.float32), "tp", 0
    )
    hidden = normalize(ALPHA * tokens.astype(jnp.float32) + branch, mixer_gain).astype(jnp.bfloat16)
    hidden_all = gather_directly(hidden, "tp", 0)
    piece = hidden_all
    upward = sent_and_summed(jnp.dot(piece, up_weight, preferred_element_type=jnp.float32), KV, 0)
    active = jnp.square(jax.nn.relu(upward)).astype(jnp.bfloat16)
    terms = jnp.dot(gather_directly(active, KV, 0), down_weight, preferred_element_type=jnp.float32)
    downward = sent_and_summed(terms, "tp", 0)
    result = normalize(ALPHA * hidden.astype(jnp.float32) + downward, final_gain)
    return result.astype(jnp.bfloat16)


def solution(mesh):
    finer = Mesh(mesh.devices.reshape(4, 4, mesh.shape["tp"]), ("kv_0", "kv_1", "tp"))
    placed = (
        P("tp", KV),
        P(KV),
        P(KV, None, "tp"),
        P(KV, None, "tp"),
        P(KV, None, "tp"),
        P(KV, "tp"),
        P(KV, "tp"),
        P(KV, "tp"),
        P(KV, "tp"),
        P("tp"),
        P("tp"),
        P("tp", KV),
        P(KV),
        P(KV, "tp"),
        P("tp", KV),
        P(KV),
    )
    return jax.shard_map(
        per_device, mesh=finer, in_specs=placed, out_specs=P("tp", KV), check_vma=False
    )
```

profile of v0, /device:TPU:2, one launch (start us, length us, event | category | flops | bytes accessed | tf_op | source)
XLA Modules:
  0.0 297.4 jit_solution(9212659954619305765)
XLA Ops:
  0.0 0.9 broadcast_in_dim.16
  0.9 24.4 %all_to_all.40 = bf16[16,64,256]{2,1,0:T(8,128)(2,1)S(1)} all-to-all(bf16[16,64,256]{2,1,0:T(8,128)(2,1)S(1)} %broadcast_in_dim.16), channel_id=1, replica_groups=mesh['kv_0'=4,'kv_1'=4,'tp'=16] {'tp'}, dimensions={0} | all-to-all | bytes 1048576 | tf_op jit(solution)/shard_map/all_to_all | solution.py:24
  25.3 1.1 fusion.26
  26.5 0.3 fusion.25
  26.8 0.3 fusion.24
  27.1 0.3 fusion.23
  27.6 1.9 copy.23
  29.5 7.6 %all-to-all-start.1 = ((f32[16,64,512]{2,1,0:T(8,128)}), f32[16,64,512]{2,1,0:T(8,128)S(1)}, u32[]{:S(2)}, u32[]{:S(2)}) async-start(f32[16,64,512]{2,1,0:T(8,128)} %bitcast.40), calls=%async_computation.1 | async-start | bytes 4194304 | tf_op jit(solution)/shard_map/all_to_all | solution.py:46
  37.4 5.1 %reshape.219 = bf16[64,64,2,64]{3,2,1,0:T(2,128)(2,1)} reshape(f32[64,64,128]{2,1,0:T(8,128)} %param.18) | data formatting | bytes 3145728 | tf_op jit(solution)/shard_map/reshape | solution.py:96
  42.5 4.1 %copy.24 = bf16[64,128,128]{1,2,0:T(8,128)(2,1)} copy(bf16[64,128,128]{2,1,0:T(8,128)(2,1)} %param.19) | data formatting | bytes 4194304 | tf_op args[3]
  46.6 4.1 %copy.25 = bf16[64,128,128]{1,2,0:T(8,128)(2,1)} copy(bf16[64,128,128]{2,1,0:T(8,128)(2,1)} %param.20) | data formatting | bytes 4194304 | tf_op args[4]
  51.1 16.0 %all-to-all-done.1 = f32[16,64,512]{2,1,0:T(8,128)S(1)} async-done(((f32[16,64,512]{2,1,0:T(8,128)}), f32[16,64,512]{2,1,0:T(8,128)S(1)}, u32[]{:S(2)}, u32[]{:S(2)}) %all-to-all-start.1) | async-done | bytes 2097184 | tf_op jit(solution)/shard_map/all_to_all | solution.py:46
  67.8 0.3 fusion.10
  68.4 2.4 fusion
  70.7 0.7 fusion.15
  71.6 1.2 fusion.11
  72.7 0.3 fusion.22
  73.7 16.0 %all_to_all.41 = bf16[16,64,128]{2,1,0:T(8,128)(2,1)S(1)} all-to-all(bf16[16,64,128]{2,1,0:T(8,128)(2,1)S(1)} %broadcast_in_dim.19), channel_id=1, replica_groups=mesh['kv_0'=4,'kv_1'=4,'tp'=16] {'kv_0','kv_1'}, dimensions={0} | all-to-all | bytes 524288 | tf_op jit(solution)/shard_map/all_to_all | solution.py:24
  89.6 0.3 fusion.8
  89.9 29.8 %all_to_all.42 = f32[16,64,256]{2,1,0:T(8,128)S(1)} all-to-all(f32[16,64,256]{2,1,0:T(8,128)S(1)} %fusion.8), channel_id=1, replica_groups=mesh['kv_0'=4,'kv_1'=4,'tp'=16] {'tp'}, dimensions={0} | all-to-all | bytes 2097152 | tf_op jit(solution)/shard_map/all_to_all | solution.py:46
  119.9 8.6 %all-reduce.3 = (f32[64]{0:T(128)S(1)}, f32[64]{0:T(128)S(1)}) all-reduce(f32[64]{0:T(128)S(1)} %get-tuple-element.8, f32[64]{0:T(128)S(1)} %get-tuple-element.7), channel_id=1, replica_groups=mesh['kv_0'=4,'kv_1'=4,'tp'=16] {'kv_0'}, use_global_device_ids=true, to_apply=%region_8.9 | all-reduce | flops 128 | bytes 1024 | tf_op jit(solution)/shard_map/psum | solution.py:19
  128.5 9.2 %all-reduce.1 = (f32[64]{0:T(128)S(1)}, f32[64]{0:T(128)S(1)}) all-reduce(f32[64]{0:T(128)S(1)} %get-tuple-element.15, f32[64]{0:T(128)S(1)} %get-tuple-element.16), channel_id=1, replica_groups=mesh['kv_0'=4,'kv_1'=4,'tp'=16] {'kv_1'}, use_global_device_ids=true, to_apply=%region_9.10 | all-reduce | flops 128 | bytes 1024 | tf_op jit(solution)/shard_map/psum | solution.py:19
  137.8 20.0 %all_to_all.43 = bf16[16,64,256]{2,1,0:T(8,128)(2,1)S(1)} all-to-all(bf16[16,64,256]{2,1,0:T(8,128)(2,1)S(1)} %broadcast_in_dim.20), channel_id=1, replica_groups=mesh['kv_0'=4,'kv_1'=4,'tp'=16] {'tp'}, dimensions={0} | all-to-all | bytes 1048576 | tf_op jit(solution)/shard_map/all_to_all | solution.py:24
  157.8 0.7 fusion.4
  158.5 54.7 %all_to_all.44 = f32[16,64,1024]{2,1,0:T(8,128)} all-to-all(f32[16,64,1024]{2,1,0:T(8,128)S(1)} %fusion.4), channel_id=1, replica_groups=mesh['kv_0'=4,'kv_1'=4,'tp'=16] {'kv_0','kv_1'}, dimensions={0} | all-to-all | bytes 8388608 | tf_op jit(solution)/shard_map/all_to_all | solution.py:46
  213.2 2.5 reduce_sum.96
  216.0 32.3 %all_to_all.45 = bf16[16,64,1024]{2,1,0:T(8,128)(2,1)S(1)} all-to-all(bf16[16,64,1024]{2,1,0:T(8,128)(2,1)S(1)} %broadcast_in_dim.21), channel_id=1, replica_groups=mesh['kv_0'=4,'kv_1'=4,'tp'=16] {'kv_0','kv_1'}, dimensions={0} | all-to-all | bytes 4194304 | tf_op jit(solution)/shard_map/all_to_all | solution.py:24
  248.3 0.7 fusion.2
  249.0 29.8 %all_to_all.46 = f32[16,64,256]{2,1,0:T(8,128)S(1)} all-to-all(f32[16,64,256]{2,1,0:T(8,128)S(1)} %fusion.2), channel_id=1, replica_groups=mesh['kv_0'=4,'kv_1'=4,'tp'=16] {'tp'}, dimensions={0} | all-to-all | bytes 2097152 | tf_op jit(solution)/shard_map/all_to_all | solution.py:46
  279.0 8.6 %all-reduce.2 = (f32[64]{0:T(128)S(1)}, f32[64]{0:T(128)S(1)}) all-reduce(f32[64]{0:T(128)S(1)} %get-tuple-element.6, f32[64]{0:T(128)S(1)} %get-tuple-element.5), channel_id=1, replica_groups=mesh['kv_0'=4,'kv_1'=4,'tp'=16] {'kv_0'}, use_global_device_ids=true, to_apply=%region_16.17 | all-reduce | flops 128 | bytes 1024 | tf_op jit(solution)/shard_map/psum | solution.py:19
  287.5 9.2 %all-reduce = (f32[64]{0:T(128)S(1)}, f32[64]{0:T(128)S(1)}) all-reduce(f32[64]{0:T(128)S(1)} %get-tuple-element.13, f32[64]{0:T(128)S(1)} %get-tuple-element.14), channel_id=1, replica_groups=mesh['kv_0'=4,'kv_1'=4,'tp'=16] {'kv_1'}, use_global_device_ids=true, to_apply=%region_17.18 | all-reduce | flops 128 | bytes 1024 | tf_op jit(solution)/shard_map/psum | solution.py:19
  296.7 0.7 multiply_convert_fusion.1
  (64 shorter events, 3.3 us)
Async XLA Ops:
  0.0 157.8 %copy-start = (bf16[256,1024]{1,0:T(8,128)(2,1)S(1)}, bf16[256,1024]{1,0:T(8,128)(2,1)}, u32[]{:S(2)}) copy-start(bf16[256,1024]{1,0:T(8,128)(2,1)} %param.29) | copy-start | bytes 1572868
  0.0 26.5 %copy-start.5 = (bf16[256,128]{1,0:T(8,128)(2,1)S(1)}, bf16[256,128]{1,0:T(8,128)(2,1)}, u32[]{:S(2)}) copy-start(bf16[256,128]{1,0:T(8,128)(2,1)} %param.23) | copy-start | bytes 196612
  0.0 26.8 %copy-start.6 = (bf16[256,128]{1,0:T(8,128)(2,1)S(1)}, bf16[256,128]{1,0:T(8,128)(2,1)}, u32[]{:S(2)}) copy-start(bf16[256,128]{1,0:T(8,128)(2,1)} %param.22) | copy-start | bytes 196612
  0.9 26.2 %copy-start.7 = (bf16[256,128]{1,0:T(8,128)(2,1)S(1)}, bf16[256,128]{1,0:T(8,128)(2,1)}, u32[]{:S(2)}) copy-start(bf16[256,128]{1,0:T(8,128)(2,1)} %param.21) | copy-start | bytes 196612
  29.5 7.6 %copy-start.12 = (f32[2]{0:T(128)S(1)}, f32[2]{0:T(128)}, u32[]{:S(2)}) copy-start(f32[2]{0:T(128)} %param.25) | copy-start | bytes 28
  29.5 7.6 %copy-start.13 = (f32[128]{0:T(128)S(1)}, f32[128]{0:T(128)}, u32[]{:S(2)}) copy-start(f32[128]{0:T(128)} %param.26) | copy-start | bytes 1540
  29.5 7.7 %copy-start.11 = (s32[64]{0:T(128)S(1)}, s32[64]{0:T(128)}, u32[]{:S(2)}) copy-start(s32[64]{0:T(128)} %param.17) | copy-start | bytes 772
  29.5 37.6 %all-to-all-start.1 = ((f32[16,64,512]{2,1,0:T(8,128)}), f32[16,64,512]{2,1,0:T(8,128)S(1)}, u32[]{:S(2)}, u32[]{:S(2)}) async-start(f32[16,64,512]{2,1,0:T(8,128)} %bitcast.40), calls=%async_computation.1 | async-start | bytes 4194304 | tf_op jit(solution)/shard_map/all_to_all | solution.py:46
  67.2 3.5 %copy-start.2 = (bf16[64,128,128]{1,2,0:T(8,128)(2,1)S(1)}, bf16[64,128,128]{1,2,0:T(8,128)(2,1)}, u32[]{:S(2)}) copy-start(bf16[64,128,128]{1,2,0:T(8,128)(2,1)} %copy.24) | copy-start | bytes 6291460
  68.3 3.2 %copy-start.1 = (bf16[64,128,128]{1,2,0:T(8,128)(2,1)S(1)}, bf16[64,128,128]{1,2,0:T(8,128)(2,1)}, u32[]{:S(2)}) copy-start(bf16[64,128,128]{1,2,0:T(8,128)(2,1)} %copy.25) | copy-start | bytes 6291460
  71.4 18.2 %copy-start.8 = (bf16[128,256]{1,0:T(8,128)(2,1)S(1)}, bf16[128,256]{1,0:T(8,128)(2,1)}, u32[]{:S(2)}) copy-start(bf16[128,256]{1,0:T(8,128)(2,1)} %param.27) | copy-start | bytes 196612
  89.6 30.1 %copy-start.4 = (bf16[64,256]{1,0:T(8,128)(2,1)S(1)}, bf16[64,256]{1,0:T(8,128)(2,1)}, u32[]{:S(2)}) copy-start(bf16[64,256]{1,0:T(8,128)(2,1)} %param.16) | copy-start | bytes 98308
  89.6 48.0 %copy-start.9 = (f32[256]{0:T(256)S(1)}, f32[256]{0:T(256)}, u32[]{:S(2)}) copy-start(f32[256]{0:T(256)} %param.28) | copy-start | bytes 3076
  216.0 32.3 %copy-start.3 = (bf16[1024,256]{1,0:T(8,128)(2,1)S(1)}, bf16[1024,256]{1,0:T(8,128)(2,1)}, u32[]{:S(2)}) copy-start(bf16[1024,256]{1,0:T(8,128)(2,1)} %param.30) | copy-start | bytes 1572868
  249.0 47.7 %copy-start.10 = (f32[256]{0:T(256)S(1)}, f32[256]{0:T(256)}, u32[]{:S(2)}) copy-start(f32[256]{0:T(256)} %param.31) | copy-start | bytes 3076
where the time goes:
time: 298 us; the launch traced here: 297 us
  blocking collectives  242 us (81%)
  local copies, waits for them, and re-layouts  17.1 us (6%)
  waiting for transfers between devices  16 us (5%)
  matrix products  7.98 us (3%)
  starting transfers between devices  7.61 us (3%)
  other arithmetic  5.97 us (2%)
    all_to_all x3, blocking collectives, sent_and_summed(): lax.all_to_all(parts, axis, split_axis=0, concat_axis=0, tiled=True)  114 us
    all_to_all x4, blocking collectives, copy_for_each(): lax.all_to_all(jnp.broadcast_to(x[None], (peers, *x.shape)), axis, 0, 0,...  92.6 us
    psum x4, blocking collectives, by_axis(): return functools.reduce(lax.psum, axes, x)  35.5 us
    all_to_all x1, waiting for transfers between devices, sent_and_summed(): lax.all_to_all(parts, axis, split_axis=0, concat_axis=0, tiled=True)  16 us
    unnamed x30, local copies, waits for them, and re-layouts  8.22 us
    all_to_all x1, starting transfers between devices, sent_and_summed(): lax.all_to_all(parts, axis, split_axis=0, concat_axis=0, tiled=True)  7.61 us
  transfers between devices with their start and end apart: 1, of which 1 were waited for; matrix products, arithmetic and copies ran while one was open for 5% of the time, Pallas kernels for 0%

commit v1 on v0

--- a/solution.py
+++ b/solution.py
@@ -8,15 +8,14 @@
 
 HDIM = 64
 BLK = 128
-KV = ("kv_0", "kv_1")
-
+KV = ("y", "xh", "xl")
+KV_ROWS = ("xl", "y", "xh")
+TP = ("z", "c")
 
 ALPHA = 2.0**0.5
 EPS = 1e-05
-
-
-def by_axis(x, axes):
-    return functools.reduce(lax.psum, axes, x)
+F32 = jnp.float32
+BF16 = jnp.bfloat16
 
 
 def copy_for_each(x, axis):
@@ -24,27 +23,32 @@
     return lax.all_to_all(jnp.broadcast_to(x[None], (peers, *x.shape)), axis, 0, 0, tiled=True)
 
 
-def joined_along(parts, dim):
-    parts = jnp.moveaxis(parts, 0, dim)
-    dims = parts.shape
-    return parts.reshape(*dims[:dim], dims[dim] * dims[dim + 1], *dims[dim + 2 :])
+def gather_tp(x):
+    parts = copy_for_each(x, "z")
+    both = lax.all_gather(parts, "c", tiled=False)
+    return both.reshape(-1, x.shape[1])
 
 
-def gather_directly(x, axis, dim):
-    parts = copy_for_each(x, axis)
-    return joined_along(parts, dim)
+def scatter_tp(x):
+    n = x.shape[1]
+    halves = x.reshape(2, -1, n)
+    core = lax.axis_index("c")
+    mine = lax.dynamic_index_in_dim(halves, core, 0, keepdims=False)
+    other = lax.dynamic_index_in_dim(halves, 1 - core, 0, keepdims=False).astype(BF16)
+    arrived = lax.ppermute(other, "c", [(0, 1), (1, 0)])
+    pair = (mine + arrived.astype(F32)).astype(BF16)
+    parts = lax.all_to_all(pair.reshape(8, -1, n), "z", 0, 0, tiled=True)
+    return parts.astype(F32).sum(axis=0)
 
 
-def split_up(x, dim, peers):
-    dims = x.shape
-    parts = x.reshape(*dims[:dim], peers, dims[dim] // peers, *dims[dim + 1 :])
-    return jnp.moveaxis(parts, dim, 0)
+def scatter_kv(x):
+    n = x.shape[1]
+    arrived = lax.all_to_all(x.astype(BF16).reshape(16, -1, n), KV_ROWS, 0, 0, tiled=True)
+    return arrived.astype(F32).sum(axis=0)
 
 
-def sent_and_summed(x, axis, dim):
-    parts = split_up(x, dim, lax.axis_size(axis))
-    arrived = lax.all_to_all(parts, axis, split_axis=0, concat_axis=0, tiled=True)
-    return arrived.sum(axis=0)
+def gather_kv(x):
+    return copy_for_each(x, KV_ROWS).reshape(-1, x.shape[1])
 
 
 def rotate(vectors, positions):
@@ -59,7 +63,8 @@
 
 def normalize(values, gain):
     width = values.shape[1] * lax.axis_size(KV)
-    total, square = (by_axis(jnp.sum(values, 1), KV), by_axis(jnp.sum(values * values, 1), KV))
+    sums = jnp.stack([jnp.sum(values, 1), jnp.sum(values * values, 1)])
+    total, square = lax.psum(lax.psum(sums, "y"), ("xh", "xl"))
     mean = total / width
     centred = values - mean[:, None]
     spread = square / width - mean * mean
@@ -124,20 +129,10 @@
     down_weight,
     final_gain,
 ):
-    all_rows = gather_directly(tokens, "tp", 0)
     width = query_weight.shape[1]
-    piece = all_rows
-    summed = sent_and_summed(
-        jnp.concatenate(
-            [
-                jnp.dot(piece, weight, preferred_element_type=jnp.float32)
-                for weight in (query_weight, key_weight, value_weight, gate_weight)
-            ],
-            1,
-        ),
-        KV,
-        0,
-    ).astype(jnp.bfloat16)
+    joined = jnp.concatenate([query_weight, key_weight, value_weight, gate_weight], 1)
+    all_rows = gather_tp(tokens)
+    summed = scatter_kv(jnp.dot(all_rows, joined, preferred_element_type=F32)).astype(BF16)
     query, keyed, valued, gated = [
         summed[:, index * width : (index + 1) * width] for index in range(4)
     ]
@@ -153,42 +148,35 @@
         decay_rate,
         head_gain,
     )
-    mixed_all = gather_directly(mixed, KV, 0)
-    piece = mixed_all
-    branch = sent_and_summed(
-        jnp.dot(piece, out_weight, preferred_element_type=jnp.float32), "tp", 0
-    )
-    hidden = normalize(ALPHA * tokens.astype(jnp.float32) + branch, mixer_gain).astype(jnp.bfloat16)
-    hidden_all = gather_directly(hidden, "tp", 0)
-    piece = hidden_all
-    upward = sent_and_summed(jnp.dot(piece, up_weight, preferred_element_type=jnp.float32), KV, 0)
-    active = jnp.square(jax.nn.relu(upward)).astype(jnp.bfloat16)
-    terms = jnp.dot(gather_directly(active, KV, 0), down_weight, preferred_element_type=jnp.float32)
-    downward = sent_and_summed(terms, "tp", 0)
-    result = normalize(ALPHA * hidden.astype(jnp.float32) + downward, final_gain)
-    return result.astype(jnp.bfloat16)
+    branch = scatter_tp(jnp.dot(gather_kv(mixed), out_weight, preferred_element_type=F32))
+    hidden = normalize(ALPHA * tokens.astype(F32) + branch, mixer_gain).astype(BF16)
+    upward = scatter_kv(jnp.dot(gather_tp(hidden), up_weight, preferred_element_type=F32))
+    active = jnp.square(jax.nn.relu(upward)).astype(BF16)
+    downward = scatter_tp(jnp.dot(gather_kv(active), down_weight, preferred_element_type=F32))
+    result = normalize(ALPHA * hidden.astype(F32) + downward, final_gain)
+    return result.astype(BF16)
 
 
 def solution(mesh):
-    finer = Mesh(mesh.devices.reshape(4, 4, mesh.shape["tp"]), ("kv_0", "kv_1", "tp"))
+    finer = Mesh(mesh.devices.reshape(4, 2, 2, 8, 2), ("y", "xh", "xl", "z", "c"))
     placed = (
-        P("tp", KV),
+        P(TP, KV),
         P(KV),
-        P(KV, None, "tp"),
-        P(KV, None, "tp"),
-        P(KV, None, "tp"),
-        P(KV, "tp"),
-        P(KV, "tp"),
-        P(KV, "tp"),
-        P(KV, "tp"),
-        P("tp"),
-        P("tp"),
-        P("tp", KV),
+        P(KV, None, TP),
+        P(KV, None, TP),
+        P(KV, None, TP),
+        P(KV, TP),
+        P(KV, TP),
+        P(KV, TP),
+        P(KV, TP),
+        P(TP),
+        P(TP),
+        P(TP, KV),
         P(KV),
-        P(KV, "tp"),
-        P("tp", KV),
+        P(KV, TP),
+        P(TP, KV),
         P(KV),
     )
     return jax.shard_map(
-        per_device, mesh=finer, in_specs=placed, out_specs=P("tp", KV), check_vma=False
+        per_device, mesh=finer, in_specs=placed, out_specs=P(TP, KV), check_vma=False
     )

time: 298 us -> 222 us (0.74)
  blocking collectives: 242 us -> 145 us
  starting transfers between devices: 7.61 us -> 22.2 us
  waiting for transfers between devices: 16 us -> 21.8 us
    all_to_all x3, blocking collectives: 114 us -> 60.9 us  [the longest x1 31.2 us: scatter_kv(): lax.all_to_all(x.astype(BF16).reshape(16, -1, n), KV_ROWS, 0, 0, tiled=True)]
    all_to_all x4 -> x2, blocking collectives: 92.6 us -> 43.5 us  [copy_for_each(): lax.all_to_all(jnp.broadcast_to(x[None], (peers, *x.shape)), axis, 0, 0,...]
    all_to_all x1 -> x3, starting transfers between devices: 7.61 us -> 22 us  [the longest x2 14.5 us: copy_for_each(): lax.all_to_all(jnp.broadcast_to(x[None], (peers, *x.shape)), axis, 0, 0,...]
    all_gather x0 -> x2, blocking collectives: none -> 4.34 us  [gather_tp(): both = lax.all_gather(parts, 'c', tiled=False)]
    ppermute x0 -> x2, waiting for transfers between devices: none -> 3.04 us  [scatter_tp(): arrived = lax.ppermute(other, 'c', [(0, 1), (1, 0)])]
    all_to_all x1 -> x3, waiting for transfers between devices: 16 us -> 18.7 us  [the longest x2 17 us: copy_for_each(): lax.all_to_all(jnp.broadcast_to(x[None], (peers, *x.shape)), axis, 0, 0,...]
    unnamed x30 -> x18, local copies, waits for them, and re-layouts: 8.22 us -> 8.2 us
  transfers between devices with their start and end apart: 1 -> 5, of which waited for: 1 -> 5; matrix products, arithmetic and copies ran while one was open for 5% -> 7% of each run, Pallas kernels for 0% -> 0%
where the time goes in v1:
time: 222 us; the launch traced here: 220 us
  blocking collectives  145 us (65%)
  starting transfers between devices  22.2 us (10%)
  waiting for transfers between devices  21.8 us (10%)
  local copies, waits for them, and re-layouts  18.6 us (8%)
  matrix products  7.34 us (3%)
  other arithmetic  5.2 us (2%)
    all_to_all x2, blocking collectives, copy_for_each(): lax.all_to_all(jnp.broadcast_to(x[None], (peers, *x.shape)), axis, 0, 0,...  43.5 us
    psum x4, blocking collectives, normalize(): total, square = lax.psum(lax.psum(sums, 'y'), ('xh', 'xl'))  36.1 us
    all_to_all x1, blocking collectives, scatter_kv(): lax.all_to_all(x.astype(BF16).reshape(16, -1, n), KV_ROWS, 0, 0, tiled=True)  31.2 us
    all_to_all x2, blocking collectives, scatter_tp(): parts = lax.all_to_all(pair.reshape(8, -1, n), 'z', 0, 0, tiled=True)  29.7 us
    all_to_all x2, waiting for transfers between devices, copy_for_each(): lax.all_to_all(jnp.broadcast_to(x[None], (peers, *x.shape)), axis, 0, 0,...  17 us
    all_to_all x2, starting transfers between devices, copy_for_each(): lax.all_to_all(jnp.broadcast_to(x[None], (peers, *x.shape)), axis, 0, 0,...  14.5 us
    unnamed x18, local copies, waits for them, and re-layouts  8.2 us
    all_to_all x1, starting transfers between devices, scatter_kv(): lax.all_to_all(x.astype(BF16).reshape(16, -1, n), KV_ROWS, 0, 0, tiled=True)  7.48 us
  transfers between devices with their start and end apart: 5, of which 5 were waited for; matrix products, arithmetic and copies ran while one was open for 7% of the time, Pallas kernels for 0%

profile of v1, /device:TPU:2, one launch (start us, length us, event | category | flops | bytes accessed | tf_op | source)
XLA Modules:
  0.0 220.3 jit_solution(17908116493295890679)
XLA Ops:
  0.0 1.5 broadcast_in_dim.16
  1.5 8.5 %all-to-all-start = ((bf16[8,64,256]{2,1,0:T(8,128)(2,1)}), bf16[8,64,256]{2,1,0:T(8,128)(2,1)S(1)}, u32[]{:S(2)}, u32[]{:S(2)}) async-start(bf16[8,64,256]{2,1,0:T(8,128)(2,1)} %broadcast_in_dim.16), calls=%async_computation | async-start | bytes 524288 | tf_op jit(solution)/shard_map/all_to_all | solution.py:23
  10.7 0.7 mul.251
  11.4 0.7 add_convert_fusion.1
  12.1 9.7 %all-to-all-done = bf16[8,64,256]{2,1,0:T(8,128)(2,1)S(1)} async-done(((bf16[8,64,256]{2,1,0:T(8,128)(2,1)}), bf16[8,64,256]{2,1,0:T(8,128)(2,1)S(1)}, u32[]{:S(2)}, u32[]{:S(2)}) %all-to-all-start) | async-done | bytes 262176 | tf_op jit(solution)/shard_map/all_to_all | solution.py:23
  21.9 2.2 all-gather
  24.0 1.4 fusion.2
  25.5 1.4 copy.23
  26.8 7.5 %all-to-all-start.1 = ((bf16[16,64,512]{2,1,0:T(8,128)(2,1)}), bf16[16,64,512]{2,1,0:T(8,128)(2,1)S(1)}, u32[]{:S(2)}, u32[]{:S(2)}) async-start(bf16[16,64,512]{2,1,0:T(8,128)(2,1)} %bitcast.2), calls=%async_computation.1 | async-start | bytes 2097152 | tf_op jit(solution)/shard_map/all_to_all | solution.py:46
  34.5 5.2 %reshape.267 = bf16[64,64,2,64]{3,2,1,0:T(2,128)(2,1)} reshape(f32[64,64,128]{2,1,0:T(8,128)} %param.18) | data formatting | bytes 3145728 | tf_op jit(solution)/shard_map/reshape | solution.py:101
  39.6 4.1 %copy.24 = bf16[64,128,128]{1,2,0:T(8,128)(2,1)} copy(bf16[64,128,128]{2,1,0:T(8,128)(2,1)} %param.19) | data formatting | bytes 4194304 | tf_op args[3]
  43.7 4.1 %copy.25 = bf16[64,128,128]{1,2,0:T(8,128)(2,1)} copy(bf16[64,128,128]{2,1,0:T(8,128)(2,1)} %param.20) | data formatting | bytes 4194304 | tf_op args[4]
  48.2 1.7 all-to-all-done.1
  51.1 2.4 %fusion = f32[64,2,1,64]{3,2,1,0:T(1,128)S(1)} fusion(bf16[64,64,2,64]{3,2,1,0:T(2,128)(2,1)} %reshape.267, bf16[64,2,64,1]{2,1,0,3:T(2,128)(2,1)S(1)} %fusion.36), kind=kOutput, calls=%fused_computation | convolution fusion | flops 1048576 | bytes 1097728 | tf_op jit(solution)/shard_map/shk,skhv->shv/dot_general | solution.py:100
  54.4 1.2 fusion.21
  56.4 0.7 broadcast_in_dim.19
  57.2 6.0 %all-to-all-start.2 = ((bf16[16,64,128]{2,1,0:T(8,128)(2,1)}), bf16[16,64,128]{2,1,0:T(8,128)(2,1)S(1)}, u32[]{:S(2)}, u32[]{:S(2)}) async-start(bf16[16,64,128]{2,1,0:T(8,128)(2,1)} %broadcast_in_dim.19), calls=%async_computation.2 | async-start | bytes 524288 | tf_op jit(solution)/shard_map/all_to_all | solution.py:23
  63.2 7.3 %all-to-all-done.2 = bf16[16,64,128]{2,1,0:T(8,128)(2,1)S(1)} async-done(((bf16[16,64,128]{2,1,0:T(8,128)(2,1)}), bf16[16,64,128]{2,1,0:T(8,128)(2,1)S(1)}, u32[]{:S(2)}, u32[]{:S(2)}) %all-to-all-start.2) | async-done | bytes 262176 | tf_op jit(solution)/shard_map/all_to_all | solution.py:23
  70.9 1.5 collective-permute-done
  72.5 14.9 %all_to_all.40 = bf16[8,64,256]{2,1,0:T(8,128)(2,1)S(1)} all-to-all(bf16[8,64,256]{2,1,0:T(8,128)(2,1)S(1)} %bitcast.78), channel_id=1, replica_groups=mesh['y'=4,'xh'=2,'xl'=2,'z'=8,'c'=2] {'z'}, dimensions={0} | all-to-all | bytes 524288 | tf_op jit(solution)/shard_map/all_to_all | solution.py:40
  87.5 8.9 %psum.28 = f32[2,64]{1,0:T(2,128)S(1)} all-reduce(f32[2,64]{1,0:T(2,128)S(1)} %pad_maximum_fusion.1), channel_id=1, replica_groups=mesh['y'=4,'xh'=2,'xl'=2,'z'=8,'c'=2] {'y'}, use_global_device_ids=true, to_apply=%region_6.7 | all-reduce | flops 128 | bytes 1024 | tf_op jit(solution)/shard_map/psum | solution.py:67
  96.4 9.2 %psum.29 = f32[2,64]{1,0:T(2,128)S(1)} all-reduce(f32[2,64]{1,0:T(2,128)S(1)} %psum.28), channel_id=1, replica_groups=mesh['y'=4,'xh'=2,'xl'=2,'z'=8,'c'=2] {'xh','xl'}, use_global_device_ids=true, to_apply=%region_7.8 | all-reduce | flops 128 | bytes 1024 | tf_op jit(solution)/shard_map/psum | solution.py:67
  105.7 12.9 %all_to_all.41 = bf16[8,64,256]{2,1,0:T(8,128)(2,1)S(1)} all-to-all(bf16[8,64,256]{2,1,0:T(8,128)(2,1)S(1)} %broadcast_in_dim.20), channel_id=1, replica_groups=mesh['y'=4,'xh'=2,'xl'=2,'z'=8,'c'=2] {'z'}, dimensions={0} | all-to-all | bytes 524288 | tf_op jit(solution)/shard_map/all_to_all | solution.py:23
  118.6 2.2 all-gather.1
  120.8 0.7 convolution_convert_fusion
  121.5 31.2 %all_to_all.42 = bf16[16,64,1024]{2,1,0:T(8,128)(2,1)S(1)} all-to-all(bf16[16,64,1024]{2,1,0:T(8,128)(2,1)S(1)} %bitcast.72), channel_id=1, replica_groups=mesh['y'=4,'xh'=2,'xl'=2,'z'=8,'c'=2] {'xl','y','xh'}, dimensions={0} | all-to-all | bytes 4194304 | tf_op jit(solution)/shard_map/all_to_all | solution.py:46
  153.4 30.6 %all_to_all.43 = bf16[16,64,1024]{2,1,0:T(8,128)(2,1)S(1)} all-to-all(bf16[16,64,1024]{2,1,0:T(8,128)(2,1)S(1)} %broadcast_in_dim.21), channel_id=1, replica_groups=mesh['y'=4,'xh'=2,'xl'=2,'z'=8,'c'=2] {'xl','y','xh'}, dimensions={0} | all-to-all | bytes 4194304 | tf_op jit(solution)/shard_map/all_to_all | solution.py:23
  184.0 0.7 fusion.4
  184.9 1.5 collective-permute-done.1
  186.5 14.9 %all_to_all.44 = bf16[8,64,256]{2,1,0:T(8,128)(2,1)S(1)} all-to-all(bf16[8,64,256]{2,1,0:T(8,128)(2,1)S(1)} %bitcast.77), channel_id=1, replica_groups=mesh['y'=4,'xh'=2,'xl'=2,'z'=8,'c'=2] {'z'}, dimensions={0} | all-to-all | bytes 524288 | tf_op jit(solution)/shard_map/all_to_all | solution.py:40
  201.5 8.9 %psum.30 = f32[2,64]{1,0:T(2,128)S(1)} all-reduce(f32[2,64]{1,0:T(2,128)S(1)} %pad_maximum_fusion.2), channel_id=1, replica_groups=mesh['y'=4,'xh'=2,'xl'=2,'z'=8,'c'=2] {'y'}, use_global_device_ids=true, to_apply=%region_12.13 | all-reduce | flops 128 | bytes 1024 | tf_op jit(solution)/shard_map/psum | solution.py:67
  210.4 9.2 %psum.31 = f32[2,64]{1,0:T(2,128)S(1)} all-reduce(f32[2,64]{1,0:T(2,128)S(1)} %psum.30), channel_id=1, replica_groups=mesh['y'=4,'xh'=2,'xl'=2,'z'=8,'c'=2] {'xh','xl'}, use_global_device_ids=true, to_apply=%region_13.14 | all-reduce | flops 128 | bytes 1024 | tf_op jit(solution)/shard_map/psum | solution.py:67
  (64 shorter events, 6.5 us)
Async XLA Ops:
  0.0 120.8 %copy-start = (bf16[256,1024]{1,0:T(8,128)(2,1)S(1)}, bf16[256,1024]{1,0:T(8,128)(2,1)}, u32[]{:S(2)}) copy-start(bf16[256,1024]{1,0:T(8,128)(2,1)} %param.29) | copy-start | bytes 1572868
  1.5 20.3 %all-to-all-start = ((bf16[8,64,256]{2,1,0:T(8,128)(2,1)}), bf16[8,64,256]{2,1,0:T(8,128)(2,1)S(1)}, u32[]{:S(2)}, u32[]{:S(2)}) async-start(bf16[8,64,256]{2,1,0:T(8,128)(2,1)} %broadcast_in_dim.16), calls=%async_computation | async-start | bytes 524288 | tf_op jit(solution)/shard_map/all_to_all | solution.py:23
  26.8 23.1 %all-to-all-start.1 = ((bf16[16,64,512]{2,1,0:T(8,128)(2,1)}), bf16[16,64,512]{2,1,0:T(8,128)(2,1)S(1)}, u32[]{:S(2)}, u32[]{:S(2)}) async-start(bf16[16,64,512]{2,1,0:T(8,128)(2,1)} %bitcast.2), calls=%async_computation.1 | async-start | bytes 2097152 | tf_op jit(solution)/shard_map/all_to_all | solution.py:46
  50.0 3.5 %copy-start.2 = (bf16[64,128,128]{1,2,0:T(8,128)(2,1)S(1)}, bf16[64,128,128]{1,2,0:T(8,128)(2,1)}, u32[]{:S(2)}) copy-start(bf16[64,128,128]{1,2,0:T(8,128)(2,1)} %copy.24) | copy-start | bytes 6291460
  51.1 3.2 %copy-start.1 = (bf16[64,128,128]{1,2,0:T(8,128)(2,1)S(1)}, bf16[64,128,128]{1,2,0:T(8,128)(2,1)}, u32[]{:S(2)}) copy-start(bf16[64,128,128]{1,2,0:T(8,128)(2,1)} %copy.25) | copy-start | bytes 6291460
  54.2 16.3 %copy-start.5 = (bf16[128,256]{1,0:T(8,128)(2,1)S(1)}, bf16[128,256]{1,0:T(8,128)(2,1)}, u32[]{:S(2)}) copy-start(bf16[128,256]{1,0:T(8,128)(2,1)} %param.27) | copy-start | bytes 196612
  57.2 30.2 %copy-start.4 = (bf16[64,256]{1,0:T(8,128)(2,1)S(1)}, bf16[64,256]{1,0:T(8,128)(2,1)}, u32[]{:S(2)}) copy-start(bf16[64,256]{1,0:T(8,128)(2,1)} %param.16) | copy-start | bytes 98308
  57.2 13.3 %all-to-all-start.2 = ((bf16[16,64,128]{2,1,0:T(8,128)(2,1)}), bf16[16,64,128]{2,1,0:T(8,128)(2,1)S(1)}, u32[]{:S(2)}, u32[]{:S(2)}) async-start(bf16[16,64,128]{2,1,0:T(8,128)(2,1)} %broadcast_in_dim.19), calls=%async_computation.2 | async-start | bytes 524288 | tf_op jit(solution)/shard_map/all_to_all | solution.py:23
  63.2 42.4 %copy-start.6 = (f32[256]{0:T(256)S(1)}, f32[256]{0:T(256)}, u32[]{:S(2)}) copy-start(f32[256]{0:T(256)} %param.28) | copy-start | bytes 3076
  70.8 1.6 collective-permute-start
  153.4 30.6 %copy-start.3 = (bf16[1024,256]{1,0:T(8,128)(2,1)S(1)}, bf16[1024,256]{1,0:T(8,128)(2,1)}, u32[]{:S(2)}) copy-start(bf16[1024,256]{1,0:T(8,128)(2,1)} %param.30) | copy-start | bytes 1572868
  184.7 34.9 %copy-start.7 = (f32[256]{0:T(256)S(1)}, f32[256]{0:T(256)}, u32[]{:S(2)}) copy-start(f32[256]{0:T(256)} %param.31) | copy-start | bytes 3076
  184.8 1.6 collective-permute-start.1
